TPU v7x, 512 devices: a whole 4x4x16 slice. The times are simulated.
512 devices in a mesh: fs: 16 (over y, x), tp: 32 (over z, core).
Axes of the slice: x: 4, y: 4, z: 16, core: 2. Of those that a mesh axis runs over, the one named last changes fastest.
Arguments:
- inputs: bfloat16 [32, 320, 2048], P('tp'), may hold values from -6 to 6
- cotangent: bfloat16 [32, 320, 2048], P('tp'), may hold values from -8 to 8
- gate_weight: bfloat16 [2048, 5632], P('tp', 'fs'), may hold values from -0.125 to 0.125
- up_weight: bfloat16 [2048, 5632], P('tp', 'fs'), may hold values from -0.125 to 0.125
- down_weight: bfloat16 [5632, 2048], P('fs', 'tp'), may hold values from -0.078125 to 0.078125
Outputs:
- input_grad: bfloat16 [32, 320, 2048], P('tp')
- down_grad: float32 [5632, 2048], P('fs', 'tp')
All inputs are finite; a program needn't handle non-finite values.
Results may differ from a plain program's by a relative error of at most 0.023.
Values may be sent and summed in bfloat16 or wider, within the bound.
No kernel may reach another device: no remote copies, remote signals or barrier semaphores. Data moves between devices by JAX's collectives and lax.ppermute only.
A program may use at most 64 MiB of HBM per device.

v0:
```python
import jax
import jax.numpy as jnp
from jax import lax
from jax.sharding import Mesh
from jax.sharding import PartitionSpec as P

TP = ("tp_0", "tp_1")


def sent_together(arrays, axis, dim, along):
    both = jnp.concatenate(arrays, axis=along)
    filled, at, gathered = (lax.all_gather(both, axis, axis=dim, tiled=True), 0, [])
    for a in arrays:
        gathered.append(lax.slice_in_dim(filled, at, at + a.shape[along], axis=along))
        at += a.shape[along]
    return tuple(gathered)


def reduced_to_own(blocks, axes, sequence):
    inside = blocks.shape[1:]
    blocks = blocks.reshape(*(lax.axis_size(a) for a in axes), *inside)
    blocks = jnp.moveaxis(blocks, sequence, range(len(axes))).reshape(-1, *inside)
    for k in sequence:
        blocks = lax.psum_scatter(blocks, axes[k], scatter_dimension=0, tiled=True)
    return blocks[0]


def split_up(x, dim, length):
    dims = x.shape
    blocks = x.reshape(*dims[:dim], length, dims[dim] // length, *dims[dim + 1 :])
    return jnp.moveaxis(blocks, dim, 0)


def scatter_axes(x, axes, sequence, dim):
    length = lax.axis_size(axes)
    return reduced_to_own(split_up(x, dim, length), axes, sequence)


def sent_and_summed(x, axis, dim):
    length = lax.axis_size(axis)
    blocks = lax.all_to_all(split_up(x, dim, length), axis, 0, 0, tiled=True)
    return jnp.sum(blocks.astype(jnp.float32), axis=0)


def laid_out(blocks, dim):
    blocks = jnp.moveaxis(blocks, 0, dim)
    dims = blocks.shape
    return blocks.reshape(*dims[:dim], dims[dim] * dims[dim + 1], *dims[dim + 2 :])


def sent_to_all(x, axis):
    copies = jnp.broadcast_to(x, (lax.axis_size(axis), *x.shape))
    return lax.all_to_all(copies, axis, split_axis=0, concat_axis=0, tiled=True)


def gather_directly(x, axis, dim):
    return laid_out(sent_to_all(x, axis), dim)


def contract_hidden(left, right):
    return lax.dot_general(
        left, right, (((1,), (1,)), ((), ())), preferred_element_type=jnp.float32
    )


def contract_tokens(left, right):
    return lax.dot_general(
        left, right, (((0,), (0,)), ((), ())), preferred_element_type=jnp.float32
    )


def per_device(inputs, cotangent, gate_weight, up_weight, down_weight):
    rows_in = inputs[0]
    rows_grad = cotangent[0]
    token_count = rows_in.shape[0]
    model_width = rows_in.shape[1]
    gate_full, up_full, down_tall = sent_together((gate_weight, up_weight, down_weight.T), TP, 0, 1)
    gate_pre = jnp.dot(rows_in, gate_full, preferred_element_type=jnp.float32)
    up_pre = jnp.dot(rows_in, up_full, preferred_element_type=jnp.float32)
    sig = jax.nn.sigmoid(gate_pre)
    hidden = (gate_pre * sig * up_pre).astype(jnp.bfloat16)
    hidden_grad = jnp.dot(rows_grad, down_tall, preferred_element_type=jnp.float32)
    gate_grad = (hidden_grad * up_pre * sig * (1.0 + gate_pre * (1.0 - sig))).astype(jnp.bfloat16)
    up_grad = (hidden_grad * gate_pre * sig).astype(jnp.bfloat16)
    partial_down = contract_tokens(hidden, rows_grad)
    down_grad = scatter_axes(partial_down.astype(jnp.bfloat16), TP, (1, 0), 1).astype(jnp.float32)
    own_sum = sent_and_summed(
        (contract_hidden(gate_grad, gate_full) + contract_hidden(up_grad, up_full)).astype(
            jnp.bfloat16
        ),
        "fs",
        0,
    )
    own_grad = own_sum.astype(jnp.bfloat16)
    whole_grad = gather_directly(own_grad, "fs", 0)
    input_grad = whole_grad.reshape(1, token_count, model_width)
    return (input_grad, down_grad)


def solution(mesh):
    finer = Mesh(mesh.devices.reshape(mesh.shape["fs"], 16, 2), ("fs", "tp_0", "tp_1"))
    return jax.shard_map(
        per_device,
        mesh=finer,
        in_specs=(P(TP, None, None), P(TP, None, None), P(TP, "fs"), P(TP, "fs"), P("fs", TP)),
        out_specs=(P(TP, None, None), P("fs", TP)),
        check_vma=False,
    )
```

profile of v0, /device:TPU:6, one launch (start us, length us, event | category | flops | bytes accessed | tf_op | source)
XLA Modules:
  0.0 200.2 jit_solution(16448081428954205659)
XLA Ops:
  7.2 0.0 copy-start
  7.2 0.0 all-gather.2.cloned.1.call-start
  7.2 1.7 concatenate.3
  8.9 0.0 all-gather.2.cloned.1.call-update
  9.0 0.0 copy-start.3
  9.0 0.0 reduce-scatter.3.cloned.1.call-start
  9.0 80.0 %all-gather.2.cloned.1.call-done = bf16[2048,1056]{1,0:T(8,128)(2,1)} async-done(((bf16[64,1056]{1,0:T(8,128)(2,1)}), bf16[2048,1056]{1,0:T(8,128)(2,1)}) %all-gather.2.cloned.1.call-update) | async-done | bytes 4325392 | tf_op jit(solution)/shard_map/all_gather | solution.py:12
  89.1 2.6 %fusion.19 = f32[320,352]{1,0:T(8,128)S(1)} fusion(bf16[2048,1056]{1,0:T(8,128)(2,1)} %all-gather.2.cloned.1.call-done, bf16[1,320,2048]{2,1,0:T(8,128)(2,1)} %param.5), kind=kOutput, calls=%fused_computation.17 | convolution fusion | flops 461373440 | bytes 3334144 | tf_op jit(solution)/shard_map/dot_general | solution.py:78
  91.7 0.0 copy-done.3
  91.7 2.5 %fusion.14 = f32[320,352]{1,0:T(8,128)S(1)} fusion(bf16[2048,1056]{1,0:T(8,128)(2,1)} %all-gather.2.cloned.1.call-done, bf16[1,320,2048]{2,1,0:T(8,128)(2,1)S(1)} %copy-done.3), kind=kOutput, calls=%fused_computation.16 | convolution fusion | flops 461373440 | bytes 3334144 | tf_op jit(solution)/shard_map/dot_general | solution.py:79
  94.3 0.0 copy-start.1
  94.3 0.8 copy-done.1
  95.0 0.0 copy-done
  95.0 2.1 %convolution_convert_fusion = bf16[352,2048]{1,0:T(8,128)(2,1)} fusion(bf16[1,320,2048]{2,1,0:T(8,128)(2,1)S(1)} %copy-done, f32[320,352]{1,0:T(8,128)S(1)} %fusion.14, f32[320,352]{1,0:T(8,128)S(1)} %fusion.19), kind=kOutput, calls=%fused_computation.1 | convolution fusion | flops 462770176 | bytes 3653632 | tf_op jit(solution)/shard_map/dot_general | solution.py:67
  97.2 1.8 copy.8
  99.0 1.3 copy.9
  100.3 0.0 reduce-scatter.3.cloned.1.call-update
  100.4 0.0 copy-start.2
  100.4 2.6 %fusion.24 = f32[320,352]{1,0:T(8,128)S(1)} fusion(bf16[2048,1056]{1,0:T(8,128)(2,1)} %all-gather.2.cloned.1.call-done, bf16[1,320,2048]{2,1,0:T(8,128)(2,1)S(1)} %copy-done), kind=kOutput, calls=%fused_computation.18 | convolution fusion | flops 461373440 | bytes 3334144 | tf_op jit(solution)/shard_map/dot_general | solution.py:82
  103.0 0.0 copy-done.2
  103.0 2.3 %fusion.3 = f32[320,2048]{1,0:T(8,128)S(1)} fusion(bf16[2048,1056]{1,0:T(8,128)(2,1)} %all-gather.2.cloned.1.call-done, f32[320,352]{1,0:T(8,128)S(1)} %fusion.19, f32[320,352]{1,0:T(8,128)S(1)} %fusion.24, f32[320,352]{1,0:T(8,128)S(1)} %copy-done.2), kind=kOutput, calls=%fused_computation.5 | convolution fusion | flops 462499840 | bytes 5545984 | tf_op jit(solution)/shard_map/dot_general | solution.py:61
  105.3 2.6 %fusion = bf16[320,2048]{1,0:T(8,128)(2,1)S(1)} fusion(f32[320,2048]{1,0:T(8,128)S(1)} %fusion.3, bf16[2048,1056]{1,0:T(8,128)(2,1)} %all-gather.2.cloned.1.call-done, f32[320,352]{1,0:T(8,128)S(1)} %fusion.24, f32[320,352]{1,0:T(8,128)S(1)} %fusion.19), kind=kOutput, calls=%fused_computation.2 | convolution fusion | flops 463360000 | bytes 6406144 | tf_op jit(solution)/shard_map/dot_general | solution.py:61
  108.0 1.3 reshape.18
  109.3 7.3 %all-to-all-start = ((bf16[16,20,2048]{2,1,0:T(8,128)(2,1)}), bf16[16,20,2048]{2,1,0:T(8,128)(2,1)S(1)}, u32[]{:S(2)}, u32[]{:S(2)}) async-start(bf16[16,20,2048]{2,1,0:T(8,128)(2,1)} %reshape.18), calls=%async_computation | async-start | bytes 3145728 | tf_op jit(solution)/shard_map/all_to_all | solution.py:41
  116.5 0.0 reduce-scatter.5.cloned.1.call-start
  116.6 0.6 reduce-scatter.3.cloned.1.call-done
  117.2 0.0 reduce-scatter.5.cloned.1.call-update
  117.3 19.9 %all-to-all-done = bf16[16,20,2048]{2,1,0:T(8,128)(2,1)S(1)} async-done(((bf16[16,20,2048]{2,1,0:T(8,128)(2,1)}), bf16[16,20,2048]{2,1,0:T(8,128)(2,1)S(1)}, u32[]{:S(2)}, u32[]{:S(2)}) %all-to-all-start) | async-done | bytes 1310752 | tf_op jit(solution)/shard_map/all_to_all | solution.py:41
  137.2 0.3 reduce_sum.12
  137.4 0.2 broadcast_in_dim.3
  137.6 27.9 %all_to_all.10 = bf16[16,20,2048]{2,1,0:T(8,128)(2,1)S(1)} all-to-all(bf16[16,20,2048]{2,1,0:T(8,128)(2,1)S(1)} %broadcast_in_dim.3), channel_id=1, replica_groups=mesh['fs'=16,'tp_0'=16,'tp_1'=2] {'fs'}, dimensions={0} | all-to-all | bytes 2621440 | tf_op jit(solution)/shard_map/all_to_all | solution.py:53
  165.5 1.2 reshape_reshape.3
  166.7 25.5 %reduce-scatter.5.cloned.1.call-done = bf16[1,352,64]{1,2,0:T(8,128)(2,1)} async-done(((bf16[16,352,64]{1,2,0:T(8,128)(2,1)}), bf16[1,352,64]{1,2,0:T(8,128)(2,1)}) %reduce-scatter.5.cloned.1.call-update) | async-done | bytes 45072 | tf_op jit(solution)/shard_map/reduce_scatter | solution.py:24
  192.2 1.4 bitcast_convert_fusion
Async XLA Ops:
  7.2 87.9 %copy-start = (bf16[1,320,2048]{2,1,0:T(8,128)(2,1)S(1)}, bf16[1,320,2048]{2,1,0:T(8,128)(2,1)}, u32[]{:S(2)}) copy-start(bf16[1,320,2048]{2,1,0:T(8,128)(2,1)} %param.6) | copy-start | bytes 3932164
  7.2 81.9 %all-gather.2.cloned.1.call-start = ((), (), s32[]{:S(2)}) async-start(), calls=%async_computation.4 | async-start | bytes 4866048 | tf_op jit(solution)/shard_map/all_gather | solution.py:12
  9.0 82.7 %copy-start.3 = (bf16[1,320,2048]{2,1,0:T(8,128)(2,1)S(1)}, bf16[1,320,2048]{2,1,0:T(8,128)(2,1)}, u32[]{:S(2)}) copy-start(bf16[1,320,2048]{2,1,0:T(8,128)(2,1)} %param.5) | copy-start | bytes 3932164
  9.0 108.3 %reduce-scatter.3.cloned.1.call-start = ((), (), s32[]{:S(2)}) async-start(), calls=%async_computation.5 | async-start | bytes 2359296 | tf_op jit(solution)/shard_map/reduce_scatter | solution.py:24
  94.3 0.8 copy-start.1
  100.4 2.6 %copy-start.2 = (f32[320,352]{1,0:T(8,128)S(1)}, f32[320,352]{1,0:T(8,128)}, u32[]{:S(2)}) copy-start(f32[320,352]{1,0:T(8,128)} %copy-done.1) | copy-start | bytes 1351684
  109.3 27.9 %all-to-all-start = ((bf16[16,20,2048]{2,1,0:T(8,128)(2,1)}), bf16[16,20,2048]{2,1,0:T(8,128)(2,1)S(1)}, u32[]{:S(2)}, u32[]{:S(2)}) async-start(bf16[16,20,2048]{2,1,0:T(8,128)(2,1)} %reshape.18), calls=%async_computation | async-start | bytes 3145728 | tf_op jit(solution)/shard_map/all_to_all | solution.py:41
  116.5 75.7 %reduce-scatter.5.cloned.1.call-start = ((), (), s32[]{:S(2)}) async-start(), calls=%async_computation.6 | async-start | bytes 835584 | tf_op jit(solution)/shard_map/reduce_scatter | solution.py:24
Sparse Core Ops, SparseCore 0:
  10.7 78.3 all-gather.1
  100.5 16.6 reduce-scatter.2
  120.1 72.0 reduce-scatter.4
where the time goes:
time: 201 us; the launch traced here: 200 us
  waiting for transfers between devices  126 us (63%)
  blocking collectives  27.9 us (14%)
  matrix products  14.8 us (7%)
  between operations  13.9 us (7%)
  local copies, waits for them, and re-layouts  8.38 us (4%)
  starting transfers between devices  7.39 us (4%)
    all_gather x1, waiting for transfers between devices, sent_together(): lax.all_gather(both, axis, axis=dim, tiled=True)  80 us
    all_to_all x1, blocking collectives, sent_to_all(): return lax.all_to_all(copies, axis, split_axis=0, concat_axis=0, tiled=True)  27.9 us
    reduce_scatter x2, waiting for transfers between devices, reduced_to_own(): blocks = lax.psum_scatter(blocks, axes[k], scatter_dimension=0, tiled=True)  26.2 us
    all_to_all x1, waiting for transfers between devices, sent_and_summed(): blocks = lax.all_to_all(split_up(x, dim, length), axis, 0, 0, tiled=True)  19.9 us
    all_to_all x1, starting transfers between devices, sent_and_summed(): blocks = lax.all_to_all(split_up(x, dim, length), axis, 0, 0, tiled=True)  7.28 us
    dot_general x2, matrix products, contract_hidden(): lax.dot_general(left, right, (((1,), (1,)), ((), ())), preferred_element_...  4.96 us
  transfers between devices with their start and end apart: 4, of which 4 were waited for; matrix products, arithmetic and copies ran while one was open for 5% of the time, Pallas kernels for 0%

commit v1 on v0

v1 whole, which is shorter than its diff:
```python
import jax
import jax.numpy as jnp
from jax import lax
from jax.sharding import Mesh
from jax.sharding import PartitionSpec as P

TP = ("zh", "zl", "c")
WEIGHT_SCALE = 2.0**18


def contract_hidden(left, right):
    return lax.dot_general(
        left, right, (((1,), (1,)), ((), ())), preferred_element_type=jnp.float32
    )


def contract_tokens(left, right):
    return lax.dot_general(
        left, right, (((0,), (0,)), ((), ())), preferred_element_type=jnp.float32
    )


def per_device(inputs, cotangent, gate_weight, up_weight, down_weight):
    rows_in = inputs[0]
    rows_grad = cotangent[0]
    tokens, width = rows_in.shape
    hid = gate_weight.shape[1]
    both = jnp.concatenate((gate_weight, up_weight, down_weight.T), axis=1)
    both = (both.astype(jnp.float32) * WEIGHT_SCALE).astype(jnp.float16)
    full = lax.all_gather(both, TP, axis=0, tiled=True)
    full = (full.astype(jnp.float32) * (1.0 / WEIGHT_SCALE)).astype(jnp.bfloat16)
    gate_full = full[:, :hid]
    up_full = full[:, hid : 2 * hid]
    down_tall = full[:, 2 * hid :]
    gate_pre = jnp.dot(rows_in, gate_full, preferred_element_type=jnp.float32)
    up_pre = jnp.dot(rows_in, up_full, preferred_element_type=jnp.float32)
    sig = jax.nn.sigmoid(gate_pre)
    hidden = (gate_pre * sig * up_pre).astype(jnp.bfloat16)
    hidden_grad = jnp.dot(rows_grad, down_tall, preferred_element_type=jnp.float32)
    gate_grad = (hidden_grad * up_pre * sig * (1.0 + gate_pre * (1.0 - sig))).astype(jnp.bfloat16)
    up_grad = (hidden_grad * gate_pre * sig).astype(jnp.bfloat16)

    term = (contract_hidden(gate_grad, gate_full) + contract_hidden(up_grad, up_full)).astype(
        jnp.bfloat16
    )
    n_fs = lax.axis_size("fs")
    pieces = term.reshape(tokens, n_fs, width // n_fs).transpose(1, 0, 2)
    parts = lax.all_to_all(pieces, "fs", 0, 0, tiled=True)
    own = jnp.sum(parts.astype(jnp.float32), axis=0).astype(jnp.bfloat16)

    zh, zl, c = (lax.axis_size(a) for a in TP)
    partial = contract_tokens(rows_grad, hidden)
    partial = partial.reshape(zh, zl, c, width // (zh * zl * c), hid)
    me = lax.axis_index("c")
    mine = lax.dynamic_index_in_dim(partial, me, 2, keepdims=False)
    other = lax.dynamic_index_in_dim(partial, 1 - me, 2, keepdims=False).astype(jnp.bfloat16)
    got = lax.ppermute(other, "c", [(0, 1), (1, 0)])
    pair = (mine + got.astype(jnp.float32)).astype(jnp.bfloat16)
    near = lax.all_to_all(pair, "zl", 1, 1, tiled=True)
    near = jnp.sum(near.astype(jnp.float32), axis=1).astype(jnp.bfloat16)
    far = lax.all_to_all(near, "zh", 0, 0, tiled=True)
    down_grad = jnp.sum(far.astype(jnp.float32), axis=0).T

    copies = jnp.broadcast_to(own, (n_fs, *own.shape))
    whole = lax.all_to_all(copies, "fs", 0, 0, tiled=True)
    input_grad = whole.transpose(1, 0, 2).reshape(1, tokens, width)
    return (input_grad, down_grad)


def solution(mesh):
    finer = Mesh(mesh.devices.reshape(mesh.shape["fs"], 4, 4, 2), ("fs", "zh", "zl", "c"))
    return jax.shard_map(
        per_device,
        mesh=finer,
        in_specs=(P(TP, None, None), P(TP, None, None), P(TP, "fs"), P(TP, "fs"), P("fs", TP)),
        out_specs=(P(TP, None, None), P("fs", TP)),
        check_vma=False,
    )
```

time: 201 us -> 159 us (0.79)
  waiting for transfers between devices: 126 us -> 49.6 us
  blocking collectives: 27.9 us -> 52.3 us
  starting transfers between devices: 7.39 us -> 27.3 us
  between operations: 13.9 us -> 0.76 us
  local copies, waits for them, and re-layouts: 8.38 us -> 15.1 us
  matrix products: 14.8 us -> 8.32 us
  other arithmetic: 1.71 us -> 4.68 us
    all_gather x1 -> x0, waiting for transfers between devices: 80 us -> none  [sent_together(): lax.all_gather(both, axis, axis=dim, tiled=True)]
    all_gather x0 -> x1, blocking collectives: none -> 52.3 us  [per_device(): full = lax.all_gather(both, TP, axis=0, tiled=True)]
    all_to_all x1 -> x0, blocking collectives: 27.9 us -> none  [sent_to_all(): return lax.all_to_all(copies, axis, split_axis=0, concat_axis=0, tiled=True)]
    all_to_all x1 -> x4, waiting for transfers between devices: 19.9 us -> 47.2 us  [the longest x1 18.8 us: per_device(): near = lax.all_to_all(pair, 'zl', 1, 1, tiled=True)]
    reduce_scatter x2 -> x0, waiting for transfers between devices: 26.2 us -> none  [reduced_to_own(): blocks = lax.psum_scatter(blocks, axes[k], scatter_dimension=0, tiled=True)]
    all_to_all x1 -> x4, starting transfers between devices: 7.28 us -> 25.4 us  [the longest x1 8.75 us: per_device(): whole = lax.all_to_all(copies, 'fs', 0, 0, tiled=True)]
    dot_general x0 -> x1, local copies, waits for them, and re-layouts: none -> 3.48 us  [contract_tokens(): lax.dot_general(left, right, (((0,), (0,)), ((), ())), preferred_element_...]
    reshape x1 -> x2, local copies, waits for them, and re-layouts: 1.31 us -> 4.64 us  [the longest x1 3.24 us: per_device(): input_grad = whole.transpose(1, 0, 2).reshape(1, tokens, width)]
  transfers between devices with their start and end apart: 4 -> 5, of which waited for: 4 -> 5; matrix products, arithmetic and copies ran while one was open for 5% -> 11% of each run, Pallas kernels for 0% -> 0%
where the time goes in v1:
time: 159 us; the launch traced here: 158 us
  blocking collectives  52.3 us (33%)
  waiting for transfers between devices  49.6 us (31%)
  starting transfers between devices  27.3 us (17%)
  local copies, waits for them, and re-layouts  15.1 us (9%)
  matrix products  8.32 us (5%)
  other arithmetic  4.68 us (3%)
    all_gather x1, blocking collectives, per_device(): full = lax.all_gather(both, TP, axis=0, tiled=True)  52.3 us
    all_to_all x1, waiting for transfers between devices, per_device(): near = lax.all_to_all(pair, 'zl', 1, 1, tiled=True)  18.8 us
    all_to_all x1, waiting for transfers between devices, per_device(): whole = lax.all_to_all(copies, 'fs', 0, 0, tiled=True)  15.8 us
    all_to_all x1, waiting for transfers between devices, per_device(): far = lax.all_to_all(near, 'zh', 0, 0, tiled=True)  10.5 us
    all_to_all x1, starting transfers between devices, per_device(): whole = lax.all_to_all(copies, 'fs', 0, 0, tiled=True)  8.75 us
    all_to_all x1, starting transfers between devices, per_device(): parts = lax.all_to_all(pieces, 'fs', 0, 0, tiled=True)  7.42 us
    all_to_all x1, starting transfers between devices, per_device(): far = lax.all_to_all(near, 'zh', 0, 0, tiled=True)  5.75 us
    dot_general x1, matrix products, contract_tokens(): lax.dot_general(left, right, (((0,), (0,)), ((), ())), preferred_element_...  3.61 us
  transfers between devices with their start and end apart: 5, of which 5 were waited for; matrix products, arithmetic and copies ran while one was open for 11% of the time, Pallas kernels for 0%

profile of v1, /device:TPU:6, one launch (start us, length us, event | category | flops | bytes accessed | tf_op | source)
XLA Modules:
  0.0 158.1 jit_solution(15377853374000755324)
XLA Ops:
  0.6 0.0 copy-start
  0.6 1.1 concatenate.3
  1.8 52.3 %all-gather.1 = f16[2048,1056]{1,0:T(8,128)(2,1)S(1)} all-gather(f16[64,1056]{1,0:T(8,128)(2,1)S(1)} %multiply_convert_fusion.4), channel_id=1, replica_groups=mesh['fs'=16,'zh'=4,'zl'=4,'c'=2] {'zh','zl','c'}, dimensions={0}, use_global_device_ids=true | all-gather | bytes 4460544 | tf_op jit(solution)/shard_map/all_gather | solution.py:30
  54.1 0.0 copy-start.2
  54.1 1.1 multiply_convert_fusion
  55.1 0.2 copy-done.2
  55.4 0.8 fusion.21
  56.2 0.9 fusion.16
  57.2 0.0 copy-done
  57.2 0.0 copy-start.1
  57.2 1.0 fusion.26
  58.1 0.0 copy-done.1
  58.2 0.9 fusion.5
  59.1 1.1 fusion.4
  60.2 1.4 copy.21
  61.6 7.4 %all-to-all-start = ((bf16[16,320,128]{2,1,0:T(8,128)(2,1)}), bf16[16,320,128]{2,1,0:T(8,128)(2,1)S(1)}, u32[]{:S(2)}, u32[]{:S(2)}) async-start(bf16[16,320,128]{2,1,0:T(8,128)(2,1)} %bitcast.44), calls=%async_computation | async-start | bytes 2621440 | tf_op jit(solution)/shard_map/all_to_all | solution.py:48
  69.0 3.6 %convolution_bitcast_fusion = f32[2048,352]{0,1:T(8,128)} fusion(bf16[1,320,2048]{2,1,0:T(8,128)(2,1)S(1)} %copy-done, f32[320,352]{1,0:T(8,128)} %copy-done.1, f32[320,352]{1,0:T(8,128)S(1)} %fusion.21), kind=kOutput, calls=%fused_computation.1 | convolution fusion | flops 462049280 | bytes 5095424 | tf_op jit(solution)/shard_map/dot_general | solution.py:18
  72.6 3.5 %copy.17 = f32[2048,352]{1,0:T(8,128)} copy(f32[2048,352]{0,1:T(8,128)} %convolution_bitcast_fusion) | data formatting | bytes 5767168 | tf_op jit(solution)/shard_map/dot_general | solution.py:18
  76.1 1.5 fusion.31
  77.6 1.9 %collective-permute-start = (bf16[4,4,64,352]{3,2,1,0:T(8,128)(2,1)S(1)}, bf16[4,4,64,352]{3,2,1,0:T(8,128)(2,1)}, u32[]{:S(2)}, u32[]{:S(2)}) collective-permute-start(bf16[4,4,64,352]{3,2,1,0:T(8,128)(2,1)S(1)} %fusion.31), channel_id=1, source_target_pairs={{0,1},{1,0},{2,3},{3,2},{4,5},{5,4},{6,7},{7,6},{8,9},{9,8},{10,11... | collective-permute-start | bytes 2162696 | tf_op jit(solution)/shard_map/ppermute | solution.py:57
  79.5 2.4 %collective-permute-done = bf16[4,4,64,352]{3,2,1,0:T(8,128)(2,1)} collective-permute-done((bf16[4,4,64,352]{3,2,1,0:T(8,128)(2,1)S(1)}, bf16[4,4,64,352]{3,2,1,0:T(8,128)(2,1)}, u32[]{:S(2)}, u32[]{:S(2)}) %collective-permute-start) | collective-permute-done | bytes 720928 | tf_op jit(solution)/shard_map/ppermute | solution.py:57
  81.9 1.8 %fusion.3 = bf16[4,4,64,352]{3,2,1,0:T(8,128)(2,1)S(1)} fusion(bf16[4,4,64,352]{3,2,1,0:T(8,128)(2,1)} %collective-permute-done, f32[4,4,2,64,352]{4,3,2,1,0:T(8,128)} %bitcast.43, s32[]{:T(128)S(6)} %select_n.7), kind=kLoop, calls=%fused_computation.7 | loop fusion | flops 1081344 | bytes 2883588 | tf_op jit(solution)/shard_map/convert_element_type | solution.py:58
  83.8 1.0 copy.18
  84.7 2.1 %all-to-all-done = bf16[16,320,128]{2,1,0:T(8,128)(2,1)S(1)} async-done(((bf16[16,320,128]{2,1,0:T(8,128)(2,1)}), bf16[16,320,128]{2,1,0:T(8,128)(2,1)S(1)}, u32[]{:S(2)}, u32[]{:S(2)}) %all-to-all-start) | async-done | bytes 1310752 | tf_op jit(solution)/shard_map/all_to_all | solution.py:48
  86.9 3.5 %all-to-all-start.2 = ((bf16[4,4,64,352]{3,2,0,1:T(8,128)(2,1)}), bf16[4,4,64,352]{3,2,0,1:T(8,128)(2,1)S(1)}, u32[]{:S(2)}, u32[]{:S(2)}) async-start(bf16[4,4,64,352]{3,2,0,1:T(8,128)(2,1)} %copy.18), calls=%async_computation.2 | async-start | bytes 1572864 | tf_op jit(solution)/shard_map/all_to_all | solution.py:59
  90.4 0.2 reduce_sum.33
  90.5 18.8 %all-to-all-done.2 = bf16[4,4,64,352]{3,2,0,1:T(8,128)(2,1)S(1)} async-done(((bf16[4,4,64,352]{3,2,0,1:T(8,128)(2,1)}), bf16[4,4,64,352]{3,2,0,1:T(8,128)(2,1)S(1)}, u32[]{:S(2)}, u32[]{:S(2)}) %all-to-all-start.2) | async-done | bytes 720928 | tf_op jit(solution)/shard_map/all_to_all | solution.py:59
  109.3 1.3 broadcast_in_dim.3
  110.6 8.8 %all-to-all-start.1 = ((bf16[16,320,128]{2,1,0:T(8,128)(2,1)}), bf16[16,320,128]{2,1,0:T(8,128)(2,1)S(1)}, u32[]{:S(2)}, u32[]{:S(2)}) async-start(bf16[16,320,128]{2,1,0:T(8,128)(2,1)} %broadcast_in_dim.3), calls=%async_computation.1 | async-start | bytes 2621440 | tf_op jit(solution)/shard_map/all_to_all | solution.py:65
  119.4 0.9 reduce_sum.34
  120.3 15.8 %all-to-all-done.1 = bf16[16,320,128]{2,1,0:T(8,128)(2,1)S(1)} async-done(((bf16[16,320,128]{2,1,0:T(8,128)(2,1)}), bf16[16,320,128]{2,1,0:T(8,128)(2,1)S(1)}, u32[]{:S(2)}, u32[]{:S(2)}) %all-to-all-start.1) | async-done | bytes 1310752 | tf_op jit(solution)/shard_map/all_to_all | solution.py:65
  136.1 5.8 %all-to-all-start.3 = ((bf16[4,64,352]{2,1,0:T(8,128)(2,1)}), bf16[4,64,352]{2,1,0:T(8,128)(2,1)S(1)}, u32[]{:S(2)}, u32[]{:S(2)}) async-start(bf16[4,64,352]{2,1,0:T(8,128)(2,1)} %reduce_sum.34), calls=%async_computation.3 | async-start | bytes 393216 | tf_op jit(solution)/shard_map/all_to_all | solution.py:61
  141.8 1.9 %copy.16 = bf16[320,16,128]{2,1,0:T(8,128)(2,1)} copy(bf16[320,16,128]{2,0,1:T(8,128)(2,1)S(1)} %bitcast.45) | data formatting | bytes 2621440 | tf_op jit(solution)/shard_map/transpose | solution.py:66
  143.7 3.2 %reshape.15 = bf16[1,320,2048]{2,1,0:T(8,128)(2,1)} reshape(bf16[320,16,128]{2,1,0:T(8,128)(2,1)} %copy.16) | data formatting | bytes 2621440 | tf_op jit(solution)/shard_map/reshape | solution.py:66
  147.0 10.5 %all-to-all-done.3 = bf16[4,64,352]{2,1,0:T(8,128)(2,1)S(1)} async-done(((bf16[4,64,352]{2,1,0:T(8,128)(2,1)}), bf16[4,64,352]{2,1,0:T(8,128)(2,1)S(1)}, u32[]{:S(2)}, u32[]{:S(2)}) %all-to-all-start.3) | async-done | bytes 180256 | tf_op jit(solution)/shard_map/all_to_all | solution.py:61
  157.5 0.7 convert_reduce_fusion
  (1 shorter events, 0.0 us)
Async XLA Ops:
  0.6 56.5 %copy-start = (bf16[1,320,2048]{2,1,0:T(8,128)(2,1)S(1)}, bf16[1,320,2048]{2,1,0:T(8,128)(2,1)}, u32[]{:S(2)}) copy-start(bf16[1,320,2048]{2,1,0:T(8,128)(2,1)} %param.6) | copy-start | bytes 3932164
  54.1 1.3 copy-start.2
  57.2 1.0 copy-start.1
  61.6 25.3 %all-to-all-start = ((bf16[16,320,128]{2,1,0:T(8,128)(2,1)}), bf16[16,320,128]{2,1,0:T(8,128)(2,1)S(1)}, u32[]{:S(2)}, u32[]{:S(2)}) async-start(bf16[16,320,128]{2,1,0:T(8,128)(2,1)} %bitcast.44), calls=%async_computation | async-start | bytes 2621440 | tf_op jit(solution)/shard_map/all_to_all | solution.py:48
  77.6 4.3 %collective-permute-start = (bf16[4,4,64,352]{3,2,1,0:T(8,128)(2,1)S(1)}, bf16[4,4,64,352]{3,2,1,0:T(8,128)(2,1)}, u32[]{:S(2)}, u32[]{:S(2)}) collective-permute-start(bf16[4,4,64,352]{3,2,1,0:T(8,128)(2,1)S(1)} %fusion.31), channel_id=1, source_target_pairs={{0,1},{1,0},{2,3},{3,2},{4,5},{5,4},{6,7},{7,6},{8,9},{9,8},{10,11... | collective-permute-start | bytes 2162696 | tf_op jit(solution)/shard_map/ppermute | solution.py:57
  86.9 22.5 %all-to-all-start.2 = ((bf16[4,4,64,352]{3,2,0,1:T(8,128)(2,1)}), bf16[4,4,64,352]{3,2,0,1:T(8,128)(2,1)S(1)}, u32[]{:S(2)}, u32[]{:S(2)}) async-start(bf16[4,4,64,352]{3,2,0,1:T(8,128)(2,1)} %copy.18), calls=%async_computation.2 | async-start | bytes 1572864 | tf_op jit(solution)/shard_map/all_to_all | solution.py:59
  110.6 25.4 %all-to-all-start.1 = ((bf16[16,320,128]{2,1,0:T(8,128)(2,1)}), bf16[16,320,128]{2,1,0:T(8,128)(2,1)S(1)}, u32[]{:S(2)}, u32[]{:S(2)}) async-start(bf16[16,320,128]{2,1,0:T(8,128)(2,1)} %broadcast_in_dim.3), calls=%async_computation.1 | async-start | bytes 2621440 | tf_op jit(solution)/shard_map/all_to_all | solution.py:65
  136.1 21.4 %all-to-all-start.3 = ((bf16[4,64,352]{2,1,0:T(8,128)(2,1)}), bf16[4,64,352]{2,1,0:T(8,128)(2,1)S(1)}, u32[]{:S(2)}, u32[]{:S(2)}) async-start(bf16[4,64,352]{2,1,0:T(8,128)(2,1)} %reduce_sum.34), calls=%async_computation.3 | async-start | bytes 393216 | tf_op jit(solution)/shard_map/all_to_all | solution.py:61
